TPU v7x, 256 devices: a whole 4x4x8 slice. The times are simulated.
256 devices in a mesh: ep: 64 (over z, x, core), tp: 4 (over y).
Axes of the slice: x: 4, y: 4, z: 8, core: 2. Of those that a mesh axis runs over, the one named last changes fastest.
Arguments:
- queries: bfloat16 [32768, 2048], P('ep', 'tp'), may hold values from -6 to 6
- keys_values: bfloat16 [32768, 4, 128], P('ep', 'tp'), may hold values from -12 to 12
- sinks: float32 [32], P('tp'), may hold values from 1 to 5
- tokens_b: bfloat16 [32768, 2048], P(('ep', 'tp')), may hold values from -6 to 6
- norm_gain: float32 [2048], replicated, may hold values from 0.1 to 1.9
- routes: int32 [32768, 2], P(('ep', 'tp')), may hold values from 0 to 63, all different within a row; in each aligned block of 128 rows (0 to 127, 128 to 255, ...) at most 5 rows name the same one
- route_weights: float32 [32768, 2], P(('ep', 'tp')), may hold values from 0.1 to 0.9
- gate_weight: bfloat16 [64, 2048, 3584], P('ep', None, 'tp'), may hold values from -0.125 to 0.125
- up_weight: bfloat16 [64, 2048, 3584], P('ep', None, 'tp'), may hold values from -0.125 to 0.125
- down_weight: bfloat16 [64, 3584, 2048], P('ep', 'tp'), may hold values from -0.09375 to 0.09375
Outputs:
- attended: bfloat16 [32768, 2048], P('ep', 'tp')
- moe_out: bfloat16 [32768, 2048], P(('ep', 'tp'))
Inputs may be any that keep to these rules, and one draw needn't show every extreme that they name: `routes`: in each aligned block of 128 rows (the rows of one device) no expert is named by more than 5 rows; the 2 entries of a row differ.
All inputs are finite; a program needn't handle non-finite values.
Results may differ from a plain program's by a relative error of at most 0.012.
Values may be sent and summed in bfloat16 or wider, within the bound.
A program may use at most 128 MiB of HBM per device.

v0:
```python
import jax
import jax.numpy as jnp
from jax import lax
from jax.sharding import PartitionSpec as P

HEADS = 32
WINDOW = 128


NEG_SCORE = -1e30
EPSILON = 1e-06


def passed_along(value, axis, by):
    size = lax.axis_size(axis)
    pairs = [(i, i + by) for i in range(size) if 0 <= i + by < size]
    return lax.ppermute(value, axis, pairs)


def split_up(value, dim, size):
    before, after = (value.shape[:dim], value.shape[dim + 1 :])
    return jnp.moveaxis(value.reshape(*before, size, -1, *after), dim, 0)


def sent_and_summed(value, axis, dim):
    parts = split_up(value, dim, lax.axis_size(axis))
    arrived = lax.all_to_all(parts, axis, split_axis=0, concat_axis=0, tiled=True)
    return arrived.astype(jnp.float32).sum(axis=0)


def window_attention(queries, keys_values, sinks):
    row_count, kv_local, doubled = keys_values.shape
    head_size = doubled // 2
    heads_local = queries.shape[1] // head_size
    group_size = heads_local // kv_local
    window_rows = WINDOW
    block_count = row_count // window_rows
    earlier = passed_along(keys_values[row_count - window_rows :], "ep", 1)
    extended = jnp.concatenate([earlier, keys_values], axis=0)
    banded = jnp.concatenate(
        [
            extended[:row_count].reshape(block_count, window_rows, kv_local, doubled),
            extended[window_rows:].reshape(block_count, window_rows, kv_local, doubled),
        ],
        axis=1,
    )
    grouped = queries.reshape(block_count, window_rows, kv_local, group_size, head_size)
    scores = jnp.einsum(
        "nqkgd,nskd->nkgqs", grouped, banded[..., :head_size], preferred_element_type=jnp.float32
    ) * head_size ** (-0.5)
    first_head = lax.axis_index("tp") * heads_local
    head_ids = (first_head + jnp.arange(heads_local, dtype=jnp.int32)).astype(jnp.float32)
    slopes = (2.0 ** (-8.0 * (head_ids + 1.0) / HEADS)).reshape(1, kv_local, group_size, 1, 1)
    query_pos = jnp.arange(window_rows, dtype=jnp.int32)[:, None]
    key_pos = jnp.arange(2 * window_rows, dtype=jnp.int32)[None, :]
    distance = window_rows + query_pos - key_pos
    offset = lax.axis_index("ep") * row_count
    key_global = (
        offset + (jnp.arange(block_count, dtype=jnp.int32)[:, None] - 1) * window_rows + key_pos
    )
    allowed = (distance >= 0)[None] & (distance < window_rows)[None] & (key_global >= 0)[:, None, :]
    scores = jnp.where(
        allowed[:, None, None], scores - slopes * distance.astype(jnp.float32), NEG_SCORE
    )
    sink_logit = sinks.reshape(1, kv_local, group_size, 1, 1)
    peak_score = jnp.maximum(jnp.max(scores, axis=-1, keepdims=True), sink_logit)
    exponent = jnp.exp(scores - peak_score)
    denominator = jnp.sum(exponent, axis=-1, keepdims=True) + jnp.exp(sink_logit - peak_score)
    weights = (exponent / denominator).astype(jnp.bfloat16)
    mixed = jnp.einsum(
        "nkgqs,nskd->nqkgd", weights, banded[..., head_size:], preferred_element_type=jnp.float32
    )
    return mixed.astype(jnp.bfloat16).reshape(row_count, heads_local * head_size)


def slot_ranks(chosen, expert_count):
    onehot = (chosen[:, :, None] == jnp.arange(expert_count, dtype=jnp.int32)).astype(jnp.int32)
    return jnp.sum(jnp.cumsum(onehot, axis=1) * onehot, axis=2) - 1


def local(
    queries,
    keys_values,
    sinks,
    tokens_b,
    norm_gain,
    routes,
    route_weights,
    gate_weight,
    up_weight,
    down_weight,
):
    attended = window_attention(queries, keys_values, sinks)
    widened = tokens_b.astype(jnp.float32)
    scale = lax.rsqrt(jnp.mean(widened * widened, axis=-1, keepdims=True) + EPSILON)
    normed = (widened * scale * norm_gain).astype(jnp.bfloat16)
    own_rows, top_count = routes.shape
    model_width = normed.shape[1]
    expert_count = lax.axis_size("ep")
    capacity = max(2, 5 * own_rows * top_count // (4 * expert_count))
    pair_count = own_rows * top_count
    own_experts = routes.reshape(pair_count)
    gate_local = gate_weight[0]
    up_local = up_weight[0]
    own_slots = slot_ranks(own_experts[None], expert_count)[0]
    table = jnp.full((expert_count * capacity,), pair_count, jnp.int32)
    table = table.at[own_experts * capacity + own_slots].set(
        jnp.arange(pair_count, dtype=jnp.int32)
    )
    padded = jnp.concatenate([normed, jnp.zeros((1, model_width), jnp.bfloat16)], axis=0)
    outgoing = padded[table // top_count].reshape(expert_count, capacity, model_width)
    arrived = lax.all_to_all(outgoing, "ep", split_axis=0, concat_axis=0, tiled=True)
    piece = lax.all_gather(arrived, "tp", axis=0, tiled=True)
    flat_rows = piece.reshape(-1, model_width)
    gate_part = jnp.dot(flat_rows, gate_local, preferred_element_type=jnp.float32)
    up_part = jnp.dot(flat_rows, up_local, preferred_element_type=jnp.float32)
    result = (jax.nn.silu(gate_part) * up_part).astype(jnp.bfloat16)
    hidden = result.reshape(piece.shape[0], capacity, gate_local.shape[1]).reshape(
        -1, gate_local.shape[1]
    )
    down_local = down_weight[0]
    summed = sent_and_summed(
        jnp.dot(hidden, down_local, preferred_element_type=jnp.float32).astype(jnp.bfloat16),
        "tp",
        0,
    ).astype(jnp.bfloat16)
    returned = lax.all_to_all(
        summed.reshape(-1, capacity, model_width), "ep", split_axis=0, concat_axis=0, tiled=True
    )
    returned = returned.reshape(-1, model_width)
    picked = returned[own_experts * capacity + own_slots].astype(jnp.float32)
    weighted = picked.reshape(own_rows, top_count, model_width) * route_weights[:, :, None]
    moe_out = jnp.sum(weighted, axis=1).astype(jnp.bfloat16)
    return (attended, moe_out)


def solution(mesh):
    in_specs = (
        P("ep", "tp"),
        P("ep", "tp", None),
        P("tp"),
        P(("ep", "tp"), None),
        P(),
        P(("ep", "tp"), None),
        P(("ep", "tp"), None),
        P("ep", None, "tp"),
        P("ep", None, "tp"),
        P("ep", "tp", None),
    )
    out_specs = (P("ep", "tp"), P(("ep", "tp"), None))
    return jax.shard_map(local, mesh=mesh, in_specs=in_specs, out_specs=out_specs, check_vma=False)
```

profile of v0, /device:TPU:1, one launch (start us, length us, event | category | flops | bytes accessed | tf_op | source)
XLA Modules:
  0.0 333.2 jit_solution(17974118181820881681)
XLA Ops:
  7.2 0.8 copy.35
  9.1 0.7 broadcast_multiply_fusion.1
  10.4 1.4 scatter_custom_fusion
  11.9 1.2 fusion.15
  13.1 1.2 fusion.17
  14.4 2.4 gather_fusion
  17.4 62.5 %all_to_all.15 = bf16[64,5,2048]{2,1,0:T(8,128)(2,1)S(1)} all-to-all(bf16[64,5,2048]{2,1,0:T(8,128)(2,1)S(1)} %reshape.351), channel_id=1, replica_groups=mesh['ep'=64,'tp'=4] {'ep'}, dimensions={0} | all-to-all | bytes 2621440 | tf_op jit(solution)/shard_map/all_to_all | solution.py:112
  79.9 1.9 copy.39
  81.8 57.3 %all-gather.2.cloned.1.call-done = bf16[256,5,2048]{2,0,1:T(8,128)(2,1)} async-done(((bf16[64,5,2048]{2,0,1:T(8,128)(2,1)}), bf16[256,5,2048]{2,0,1:T(8,128)(2,1)}) %all-gather.2.cloned.1.call-update) | async-done | bytes 5242896 | tf_op jit(solution)/shard_map/all_gather | solution.py:113
  139.1 8.9 %copy.40 = bf16[256,5,2048]{2,1,0:T(8,128)(2,1)} copy(bf16[256,5,2048]{2,0,1:T(8,128)(2,1)} %all-gather.2.cloned.1.call-done) | data formatting | bytes 10485760 | tf_op jit(solution)/shard_map/all_gather | solution.py:113
  148.0 10.0 %reshape.352 = bf16[1280,2048]{1,0:T(8,128)(2,1)} reshape(bf16[256,5,2048]{2,1,0:T(8,128)(2,1)} %copy.40) | data formatting | bytes 10485760 | tf_op jit(solution)/shard_map/reshape | solution.py:114
  158.0 10.0 %fusion.4 = f32[1280,896]{1,0:T(8,128)} fusion(bf16[1280,2048]{1,0:T(8,128)(2,1)} %reshape.352, bf16[1,2048,896]{2,1,0:T(8,128)(2,1)} %param.17), kind=kOutput, calls=%fused_computation.12 | convolution fusion | flops 4697620480 | bytes 13500416 | tf_op jit(solution)/shard_map/dot_general | solution.py:115
  168.0 17.5 %convolution_convert_fusion = bf16[1280,2048]{1,0:T(8,128)(2,1)} fusion(bf16[1,896,2048]{2,1,0:T(8,128)(2,1)} %param.19, f32[1280,896]{1,0:T(8,128)} %fusion.4, bf16[1280,2048]{1,0:T(8,128)(2,1)} %reshape.352, bf16[1,2048,896]{2,1,0:T(8,128)(2,1)} %param.18), kind=kOutput, calls=%fused_computation.3 | convolution fusion | flops 9404743680 | bytes 22413312 | tf_op jit(solution)/shard_map/dot_general | solution.py:123
  185.5 5.2 %all-to-all-start.1 = ((bf16[4,320,2048]{2,1,0:T(8,128)(2,1)}), bf16[4,320,2048]{2,1,0:T(8,128)(2,1)}, u32[]{:S(2)}, u32[]{:S(2)}) async-start(bf16[4,320,2048]{2,1,0:T(8,128)(2,1)} %bitcast.85), calls=%async_computation.1 | async-start | bytes 10485760 | tf_op jit(solution)/shard_map/all_to_all | solution.py:27
  191.3 3.8 %collective-permute-start = (bf16[128,1,128]{2,0,1:T(8,128)(2,1)}, bf16[128,1,128]{2,0,1:T(8,128)(2,1)}, u32[]{:S(2)}, u32[]{:S(2)}) collective-permute-start(bf16[128,1,128]{2,0,1:T(8,128)(2,1)} %slice.18), channel_id=1, source_target_pairs={{0,4},{4,8},{8,12},{12,16},{16,20},{20,24},{24,28},{28,32},{32,36}... | collective-permute-start | bytes 98312 | tf_op jit(solution)/shard_map/ppermute | solution.py:17
  195.5 54.5 %all-to-all-done.1 = bf16[4,320,2048]{2,1,0:T(8,128)(2,1)} async-done(((bf16[4,320,2048]{2,1,0:T(8,128)(2,1)}), bf16[4,320,2048]{2,1,0:T(8,128)(2,1)}, u32[]{:S(2)}, u32[]{:S(2)}) %all-to-all-start.1) | async-done | bytes 5242912 | tf_op jit(solution)/shard_map/all_to_all | solution.py:27
  250.1 3.6 %reduce_sum.51 = bf16[320,2048]{1,0:T(8,128)(2,1)S(1)} reduce(bf16[4,320,2048]{2,1,0:T(8,128)(2,1)} %all-to-all-done.1, bf16[]{:T(256)} %constant.73.clone.1), dimensions={0}, to_apply=%region_7.8 | reduce | flops 1966080 | bytes 6553602 | tf_op jit(solution)/shard_map/reduce_sum | solution.py:28
  253.7 1.6 reshape.354
  255.3 12.0 %all-to-all-start.2 = ((bf16[64,5,2048]{2,1,0:T(8,128)(2,1)}), bf16[64,5,2048]{2,1,0:T(8,128)(2,1)S(1)}, u32[]{:S(2)}, u32[]{:S(2)}) async-start(bf16[64,5,2048]{2,1,0:T(8,128)(2,1)} %reshape.354), calls=%async_computation.2 | async-start | bytes 4194304 | tf_op jit(solution)/shard_map/all_to_all | solution.py:127
  267.7 2.4 reshape.385
  270.1 0.7 copy.41
  270.8 1.4 pad_maximum_fusion.1
  272.2 1.0 copy.28
  273.3 2.3 fusion.6
  275.6 1.1 fusion.1
  276.8 2.1 fusion.12
  278.9 1.6 copy.48
  280.4 1.4 reshape.386
  281.8 35.2 %all-to-all-done.2 = bf16[64,5,2048]{2,1,0:T(8,128)(2,1)S(1)} async-done(((bf16[64,5,2048]{2,1,0:T(8,128)(2,1)}), bf16[64,5,2048]{2,1,0:T(8,128)(2,1)S(1)}, u32[]{:S(2)}, u32[]{:S(2)}) %all-to-all-start.2) | async-done | bytes 1310752 | tf_op jit(solution)/shard_map/all_to_all | solution.py:127
  317.6 2.3 gather_fusion.1
  320.0 2.4 reshape.357
  322.4 3.9 %multiply_reduce_fusion = bf16[128,2048]{1,0:T(8,128)(2,1)} fusion(f32[128,2,2048]{2,1,0:T(2,128)S(1)} %reshape.357, f32[128,2]{1,0:T(8,128)S(1)} %copy-done.1), kind=kLoop, calls=%fused_computation.17 | loop fusion | flops 786432 | bytes 2622464 | tf_op jit(solution)/shard_map/reduce_sum | solution.py:133
  (46 shorter events, 4.4 us)
Async XLA Ops:
  7.2 131.9 %all-gather.2.cloned.1.call-start = ((), (), s32[]{:S(2)}) async-start(), calls=%async_computation.3 | async-start | bytes 6553600 | tf_op jit(solution)/shard_map/all_gather | solution.py:113
  185.5 5.2 %copy-start = (bf16[512,1,128]{2,0,1:T(8,128)(2,1)S(1)}, bf16[512,1,128]{2,0,1:T(8,128)(2,1)}, u32[]{:S(2)}) copy-start(bf16[512,1,128]{2,0,1:T(8,128)(2,1)} %param.11) | copy-start | bytes 393220
  185.5 64.6 %all-to-all-start.1 = ((bf16[4,320,2048]{2,1,0:T(8,128)(2,1)}), bf16[4,320,2048]{2,1,0:T(8,128)(2,1)}, u32[]{:S(2)}, u32[]{:S(2)}) async-start(bf16[4,320,2048]{2,1,0:T(8,128)(2,1)} %bitcast.85), calls=%async_computation.1 | async-start | bytes 10485760 | tf_op jit(solution)/shard_map/all_to_all | solution.py:27
  191.3 79.5 %collective-permute-start = (bf16[128,1,128]{2,0,1:T(8,128)(2,1)}, bf16[128,1,128]{2,0,1:T(8,128)(2,1)}, u32[]{:S(2)}, u32[]{:S(2)}) collective-permute-start(bf16[128,1,128]{2,0,1:T(8,128)(2,1)} %slice.18), channel_id=1, source_target_pairs={{0,4},{4,8},{8,12},{12,16},{16,20},{20,24},{24,28},{28,32},{32,36}... | collective-permute-start | bytes 98312 | tf_op jit(solution)/shard_map/ppermute | solution.py:17
  255.3 14.8 %copy-start.3 = (f32[128,2]{0,1:T(2,128)S(1)}, f32[128,2]{0,1:T(2,128)}, u32[]{:S(2)}) copy-start(f32[128,2]{0,1:T(2,128)} %param.16) | copy-start | bytes 3076
  255.3 61.7 %all-to-all-start.2 = ((bf16[64,5,2048]{2,1,0:T(8,128)(2,1)}), bf16[64,5,2048]{2,1,0:T(8,128)(2,1)S(1)}, u32[]{:S(2)}, u32[]{:S(2)}) async-start(bf16[64,5,2048]{2,1,0:T(8,128)(2,1)} %reshape.354), calls=%async_computation.2 | async-start | bytes 4194304 | tf_op jit(solution)/shard_map/all_to_all | solution.py:127
  267.7 7.9 %copy-start.2 = (f32[8]{0:T(128)S(1)}, f32[8]{0:T(128)}, u32[]{:S(2)}) copy-start(f32[8]{0:T(128)} %param.12) | copy-start | bytes 100
  317.6 4.7 %copy-start.1 = (f32[128,2]{1,0:T(8,128)S(1)}, f32[128,2]{1,0:T(8,128)}, u32[]{:S(2)}) copy-start(f32[128,2]{1,0:T(8,128)} %copy.41) | copy-start | bytes 3076
Sparse Core Ops, SparseCore 0:
  82.0 57.0 all-gather.1
where the time goes:
time: 335 us; the launch traced here: 333 us
  waiting for transfers between devices  147 us (44%)
  blocking collectives  62.5 us (19%)
  local copies, waits for them, and re-layouts  41.7 us (12%)
  matrix products  31.8 us (9%)
  starting transfers between devices  21.1 us (6%)
  other arithmetic  14.7 us (4%)
  between operations  14.3 us (4%)
    all_to_all x1, blocking collectives, local(): lax.all_to_all(outgoing, 'ep', split_axis=0, concat_axis=0, tiled=True)  62.5 us
    all_gather x1, waiting for transfers between devices, local(): piece = lax.all_gather(arrived, 'tp', axis=0, tiled=True)  57.3 us
    all_to_all x1, waiting for transfers between devices, sent_and_summed(): lax.all_to_all(parts, axis, split_axis=0, concat_axis=0, tiled=True)  54.5 us
    all_to_all x1, waiting for transfers between devices, local(): lax.all_to_all(summed.reshape(-1, capacity, model_width), 'ep', split_axi...  35.2 us
    dot_general x1, matrix products, local(): jnp.dot(hidden, down_local, preferred_element_type=jnp.float32)  17.5 us
    all_to_all x1, starting transfers between devices, local(): lax.all_to_all(summed.reshape(-1, capacity, model_width), 'ep', split_axi...  12 us
    reshape x1, local copies, waits for them, and re-layouts, local(): flat_rows = piece.reshape(-1, model_width)  10 us
    dot_general x1, matrix products, local(): jnp.dot(flat_rows, gate_local, preferred_element_type=jnp.float32)  9.96 us
  transfers between devices with their start and end apart: 4, of which 3 were waited for; matrix products, arithmetic and copies ran while one was open for 6% of the time, Pallas kernels for 0%

commit v1 on v0

v1 whole, which is shorter than its diff:
```python
import functools

import jax
import jax.numpy as jnp
from jax import lax
from jax.experimental import pallas as pl
from jax.experimental.pallas import tpu as pltpu
from jax.sharding import PartitionSpec as P

HEADS = 32
WINDOW = 128
NEG_SCORE = -1e30
HEAD = 64
EPSILON = 1e-06
MESH = pl.DeviceIdType.MESH

NX, NC = 4, 2
CAP = 5
N_TP = 4
LANES = 128


PLAN = (
    "A0", "B0", "A1", "C0", "B1", "A2", "D0", "C1", "B2", "A3", "D1", "E0",
    "C2", "B3", "D2", "E1", "C3", "D3", "F0", "E2", "F1", "E3", "F2", "F3",
)


def z_orders(nz):
    return {8: (0, 1, 3, 5, 4, 6, 2, 7), 4: (0, 1, 2, 3), 2: (0, 1)}[nz]


def layer_kernel(
    nz,
    tokens_ref, gain_ref, routes_ref, rw_ref, sinks_ref, q_hbm, kv_hbm, wg_hbm, wu_hbm, wd_hbm,
    moe_ref, att_ref,
    normed, s_ref, out_t, in_t, xg, wg, wu, wd, hidden, part, r1, r2, q1, q2, f1, f2, ret_t, got_t, rows_ref, acc,
    q_ref, kv_ref, key_ref, value_ref,
    w_sem, kv_send, kv_recv, disp_send, disp_recv, ret_send, ret_recv, ag_send, ag_recv, rs_send, rs_recv,
):
    order = z_orders(nz)
    tokens, width = tokens_ref.shape
    half = width // 2
    cols = width // LANES
    ep_size = nz * NX * NC
    group = NX * NC
    chunks = max(1, nz // 2)
    per_chunk = ep_size // chunks
    rows = per_chunk * CAP
    unit = cols
    blk = CAP * unit
    chunk_t = per_chunk * blk
    ffl = wg.shape[1]

    ep = lax.axis_index("ep")
    tp = lax.axis_index("tp")
    my_z, my_x, my_c = ep // group, (ep // NC) % NX, ep % NC
    up_id = {"ep": ep, "tp": (tp + 1) % N_TP}
    dn_id = {"ep": ep, "tp": (tp + N_TP - 1) % N_TP}

    def ep_at(sign, dz, j):
        dx, dc = j // NC, j % NC
        z = (my_z + sign * dz + nz) % nz
        x = (my_x + sign * dx + NX) % NX
        c = (my_c + dc) % NC
        return {"ep": (z * NX + x) * NC + c, "tp": tp}

    def arrived(copy):
        with jax.named_scope("wait"):
            copy.wait_recv()

    barrier = pltpu.get_barrier_semaphore()

    def greet(i, carry):
        pl.semaphore_signal(barrier, inc=1, device_id={"ep": (ep + i) % ep_size, "tp": tp}, device_id_type=MESH)
        return carry

    lax.fori_loop(1, ep_size, greet, 0)
    pl.semaphore_signal(barrier, inc=1, device_id=up_id, device_id_type=MESH)
    pl.semaphore_signal(barrier, inc=1, device_id=dn_id, device_id_type=MESH)

    weight_copies = [
        pltpu.make_async_copy(wg_hbm, wg, w_sem.at[0]),
        pltpu.make_async_copy(wu_hbm, wu, w_sem.at[1]),
        pltpu.make_async_copy(wd_hbm, wd, w_sem.at[2]),
    ]
    kv_rows = kv_hbm.shape[0]
    kv_copy = pltpu.make_async_copy(kv_hbm, kv_ref.at[pl.ds(WINDOW, kv_rows)], w_sem.at[3])
    q_copy = pltpu.make_async_copy(q_hbm, q_ref, w_sem.at[4])
    kv_copy.start()
    q_copy.start()
    before = pltpu.make_async_remote_copy(
        src_ref=kv_ref.at[pl.ds(kv_rows, WINDOW)],
        dst_ref=kv_ref.at[pl.ds(0, WINDOW)],
        send_sem=kv_send,
        recv_sem=kv_recv,
        device_id={"ep": (ep + 1) % ep_size, "tp": tp},
        device_id_type=MESH,
    )

    for copy in weight_copies:
        copy.start()

    widened = tokens_ref[...].astype(jnp.float32)
    scale = lax.rsqrt(jnp.mean(widened * widened, axis=-1, keepdims=True) + EPSILON)
    normed[...] = (widened * scale * gain_ref[...]).astype(jnp.bfloat16)

    def relative_block(e):
        dz = (lax.shift_right_logical(e, 3) - my_z + nz) & (nz - 1)
        dx = ((lax.shift_right_logical(e, 1) & (NX - 1)) - my_x + NX) & (NX - 1)
        dc = ((e & (NC - 1)) + my_c) & (NC - 1)
        pos = jnp.zeros_like(e)
        for q, d in enumerate(order):
            pos = jnp.where(dz == d, q, pos)
        return pos * group + dx * NC + dc

    iota_et = lax.broadcasted_iota(jnp.int32, (LANES, tokens), 0)
    hot_t = [(routes_ref[k : k + 1, :] == iota_et).astype(jnp.float32) for k in range(2)]
    earlier_t = (
        lax.broadcasted_iota(jnp.int32, (tokens, tokens), 0) < lax.broadcasted_iota(jnp.int32, (tokens, tokens), 1)
    ).astype(jnp.bfloat16)
    count_t = jnp.dot((hot_t[0] + hot_t[1]).astype(jnp.bfloat16), earlier_t, preferred_element_type=jnp.float32)
    dest_t = []
    for k in range(2):
        rank = jnp.sum(hot_t[k] * count_t, axis=0, keepdims=True).astype(jnp.int32)
        dest_t.append(relative_block(routes_ref[k : k + 1, :]) * CAP + rank)

    diagonal = lax.broadcasted_iota(jnp.int32, (tokens, tokens), 0) == lax.broadcasted_iota(jnp.int32, (tokens, tokens), 1)

    def as_column(row):
        return jnp.sum(jnp.where(diagonal, row, 0.0), axis=1, keepdims=True)

    dest = [as_column(d.astype(jnp.float32)).astype(jnp.int32) for d in dest_t]
    gains = [as_column(rw_ref[k : k + 1, :]) for k in range(2)]

    col_step = min(512, width)
    groups = col_step // LANES

    def store_tiles(value, start, target, row0):
        for g in range(value.shape[1] // LANES):
            target[pl.ds(row0 + start // LANES + g, rows, stride=unit), :] = value[:, g * LANES : (g + 1) * LANES]

    def send_blocks(c, source, target, sign, send_sem, recv_sem):
        for q in range(2):
            dz = order[2 * c + q]
            first = 1 if dz == 0 else 0

            def one(j, carry, q=q, dz=dz):
                at = pl.multiple_of(((2 * c + q) * group + j) * blk, blk)
                pltpu.make_async_remote_copy(
                    src_ref=source.at[pl.ds(at, blk)],
                    dst_ref=target.at[pl.ds(at, blk)],
                    send_sem=send_sem.at[c],
                    recv_sem=recv_sem.at[c],
                    device_id=ep_at(sign, dz, j),
                    device_id_type=MESH,
                ).start()
                return carry

            lax.fori_loop(first, group, one, 0)
        if order[2 * c] == 0:
            target[c * chunk_t : c * chunk_t + blk, :] = source[c * chunk_t : c * chunk_t + blk, :]

    def chunk_copy(c, source, target, send_sem, recv_sem):
        first = blk if order[2 * c] == 0 else 0
        span = pl.ds(c * chunk_t + first, chunk_t - first)
        return pltpu.make_async_remote_copy(
            src_ref=source.at[span],
            dst_ref=target.at[span],
            send_sem=send_sem.at[c],
            recv_sem=recv_sem.at[c],
            device_id=up_id,
            device_id_type=MESH,
        )

    for c in range(chunks):
        slot = lax.broadcasted_iota(jnp.int32, (rows, tokens), 0) + c * rows
        take = ((dest_t[0] == slot) | (dest_t[1] == slot)).astype(jnp.bfloat16)
        for start in range(0, width, col_step):
            picked = jnp.dot(take, normed[:, start : start + col_step], preferred_element_type=jnp.float32)
            store_tiles(picked, start, s_ref, 0)
        out_t[c * chunk_t : (c + 1) * chunk_t, :] = s_ref[...].astype(jnp.bfloat16)
        if c == 0:
            with jax.named_scope("barrier"):
                pl.semaphore_wait(barrier, ep_size - 1 + 2)
        with jax.named_scope("send%d" % c):
            send_blocks(c, out_t, in_t, 1, disp_send, disp_recv)
        if c == 0:
            kv_copy.wait()
            before.start()

    def attention():
        q_copy.wait()
        before.wait_recv()
        wide = kv_ref[...].astype(jnp.float32)
        flip = pltpu.roll(wide, HEAD, 1)
        lane = lax.broadcasted_iota(jnp.int32, wide.shape, 1)
        key_ref[0] = jnp.where(lane < HEAD, wide, 0.0).astype(jnp.bfloat16)
        key_ref[1] = jnp.where(lane >= HEAD, flip, 0.0).astype(jnp.bfloat16)
        value_ref[0] = jnp.where(lane < HEAD, flip, 0.0).astype(jnp.bfloat16)
        value_ref[1] = jnp.where(lane >= HEAD, wide, 0.0).astype(jnp.bfloat16)
        span = 2 * WINDOW
        shape = (WINDOW, span)
        key_pos = lax.broadcasted_iota(jnp.int32, shape, 1)
        distance = WINDOW + lax.broadcasted_iota(jnp.int32, shape, 0) - key_pos
        in_band = (distance >= 0) & (distance < WINDOW)
        distance = distance.astype(jnp.float32)
        pairs = q_ref.shape[1] // LANES

        def one(i, carry):
            n, pair = i // pairs, i % pairs
            rows_at = pl.ds(pl.multiple_of(n * WINDOW, WINDOW), WINDOW)
            keys_at = pl.ds(pl.multiple_of(n * WINDOW, WINDOW), span)
            lanes_at = pl.ds(pl.multiple_of(pair * LANES, LANES), LANES)
            q = q_ref[rows_at, lanes_at]
            first_key = jnp.where(ep * kv_rows + n == 0, WINDOW, 0)
            allowed = in_band & (key_pos >= first_key)
            total = None
            for odd in range(2):
                head = tp * (2 * pairs) + 2 * pair + odd
                power = jnp.full((1, span), (head + 1).astype(jnp.float32) * (-8.0 / HEADS), jnp.float32)
                score = lax.dot_general(
                    q, key_ref[odd, keys_at, :], (((1,), (1,)), ((), ())), preferred_element_type=jnp.float32
                ) * HEAD ** (-0.5)
                score = jnp.where(allowed, score - jnp.exp2(power) * distance, NEG_SCORE)
                sink = sinks_ref[2 * pair + odd]
                peak = jnp.maximum(jnp.max(score, axis=1, keepdims=True), sink)
                exponent = jnp.exp(score - peak)
                denominator = jnp.sum(exponent, axis=1, keepdims=True) + jnp.exp(sink - peak)
                weight = (exponent * (1.0 / denominator)).astype(jnp.bfloat16)
                mixed = jnp.dot(weight, value_ref[odd, keys_at, :], preferred_element_type=jnp.float32)
                total = mixed if total is None else total + mixed
            att_ref[rows_at, lanes_at] = total.astype(jnp.bfloat16)
            return carry

        lax.fori_loop(0, (kv_rows // WINDOW) * pairs, one, 0)

    def y_copy(source, target, sems, at, device):
        send, recv = sems
        return pltpu.make_async_remote_copy(
            src_ref=source, dst_ref=target, send_sem=send.at[at], recv_sem=recv.at[at],
            device_id=device, device_id_type=MESH,
        )

    AG, RS = (ag_send, ag_recv), (rs_send, rs_recv)
    LOW, HIGH = pl.ds(0, half), pl.ds(half, half)

    def ag_up(c):
        return y_copy(xg.at[c, 0], xg.at[c, 1], AG, 4 * c, up_id)

    def ag_dn(c):
        return y_copy(xg.at[c, 0], xg.at[c, 3], AG, 4 * c + 1, dn_id)

    def ag_up2(c):
        return y_copy(xg.at[c, 1, :, LOW], xg.at[c, 2, :, LOW], AG, 4 * c + 2, up_id)

    def ag_dn2(c):
        return y_copy(xg.at[c, 3, :, HIGH], xg.at[c, 2, :, HIGH], AG, 4 * c + 3, dn_id)

    def rs_far_up(c):
        return y_copy(part.at[c, 2, :, LOW], r1.at[c], RS, 6 * c, up_id)

    def rs_far_dn(c):
        return y_copy(part.at[c, 2, :, HIGH], r2.at[c], RS, 6 * c + 1, dn_id)

    def rs_own_up(c):
        return y_copy(part.at[c, 3, :, HIGH], f1.at[c, 1], RS, 6 * c + 2, up_id)

    def rs_own_dn(c):
        return y_copy(part.at[c, 1, :, LOW], f2.at[c, 0], RS, 6 * c + 3, dn_id)

    def rs_sum_up(c):
        return y_copy(q1.at[c], f1.at[c, 0], RS, 6 * c + 4, up_id)

    def rs_sum_dn(c):
        return y_copy(q2.at[c], f2.at[c, 1], RS, 6 * c + 5, dn_id)

    def stage_a(c):
        arrived(chunk_copy(c, out_t, in_t, disp_send, disp_recv))
        s_ref[...] = in_t[c * chunk_t : (c + 1) * chunk_t, :].astype(jnp.float32)
        for g in range(cols):
            xg[c, 0, :, g * LANES : (g + 1) * LANES] = s_ref[pl.ds(g, rows, stride=unit), :].astype(jnp.bfloat16)
        ag_up(c).start()
        ag_dn(c).start()

    def stage_b(c):
        arrived(ag_up(c))
        ag_up2(c).start()
        arrived(ag_dn(c))
        ag_dn2(c).start()

    def stage_c(c):
        arrived(ag_up2(c))
        arrived(ag_dn2(c))
        if c == 0:
            weight_copies[0].wait()
            weight_copies[1].wait()

        def gate_up(j, carry):
            at = pl.ds(pl.multiple_of(j * LANES, LANES), LANES)
            both = jnp.concatenate([wg[:, at], wu[:, at]], axis=1)
            value = jnp.dot(
                xg[c].reshape(N_TP * rows, width), both, preferred_element_type=jnp.float32
            )
            gate, up = value[:, :LANES], value[:, LANES:]
            hidden[:, at] = (gate / (1.0 + jnp.exp(-gate)) * up).astype(jnp.bfloat16)
            return carry

        lax.fori_loop(0, ffl // LANES, gate_up, 0)
        if c == 0:
            weight_copies[2].wait()

        step = min(256, width)

        def down(j, carry):
            at = pl.ds(pl.multiple_of(j * step, step), step)
            value = jnp.dot(hidden[...], wd[:, at], preferred_element_type=jnp.float32)
            part[c, :, :, at] = value.astype(jnp.bfloat16).reshape(N_TP, rows, step)
            return carry

        lax.fori_loop(0, width // step, down, 0)
        rs_far_up(c).start()
        rs_far_dn(c).start()
        rs_own_up(c).start()
        rs_own_dn(c).start()

    def stage_d(c):
        arrived(rs_far_up(c))
        q1[c] = (part[c, 3, :, :half].astype(jnp.float32) + r1[c].astype(jnp.float32)).astype(jnp.bfloat16)
        rs_sum_up(c).start()
        arrived(rs_far_dn(c))
        q2[c] = (part[c, 1, :, half:].astype(jnp.float32) + r2[c].astype(jnp.float32)).astype(jnp.bfloat16)
        rs_sum_dn(c).start()

    def stage_e(c):
        arrived(rs_own_up(c))
        arrived(rs_own_dn(c))
        arrived(rs_sum_up(c))
        arrived(rs_sum_dn(c))
        for start in range(0, width, col_step):
            h, at = start // half, start % half
            value = part[c, 0, :, start : start + col_step].astype(jnp.float32)
            value = value + f1[c, h, :, at : at + col_step].astype(jnp.float32)
            value = value + f2[c, h, :, at : at + col_step].astype(jnp.float32)
            store_tiles(value, start, s_ref, 0)
        ret_t[c * chunk_t : (c + 1) * chunk_t, :] = s_ref[...].astype(jnp.bfloat16)
        send_blocks(c, ret_t, got_t, -1, ret_send, ret_recv)

    def stage_f(c, first):
        arrived(chunk_copy(c, ret_t, got_t, ret_send, ret_recv))
        s_ref[...] = got_t[c * chunk_t : (c + 1) * chunk_t, :].astype(jnp.float32)
        for g in range(cols):
            rows_ref[:, g * LANES : (g + 1) * LANES] = s_ref[pl.ds(g, rows, stride=unit), :].astype(jnp.bfloat16)
        slot = lax.broadcasted_iota(jnp.int32, (tokens, rows), 1) + c * rows
        mix = jnp.where(dest[0] == slot, gains[0], 0.0) + jnp.where(dest[1] == slot, gains[1], 0.0)
        high = mix.astype(jnp.bfloat16)
        low = (mix - high.astype(jnp.float32)).astype(jnp.bfloat16)
        for start in range(0, width, col_step):
            picked = rows_ref[:, start : start + col_step]
            value = jnp.dot(high, picked, preferred_element_type=jnp.float32)
            value = value + jnp.dot(low, picked, preferred_element_type=jnp.float32)
            if not first:
                value = value + acc[:, start : start + col_step]
            acc[:, start : start + col_step] = value

    with jax.named_scope("attention"):
        attention()
    if chunks == 4:
        plan = PLAN
    else:
        plan = [s + str(c) for s in "ABCDEF" for c in range(chunks)]
    for step in plan:
        c = int(step[1])
        with jax.named_scope(step):
            if step[0] == "F":
                stage_f(c, c == 0)
            else:
                {"A": stage_a, "B": stage_b, "C": stage_c, "D": stage_d, "E": stage_e}[step[0]](c)
    moe_ref[...] = acc[...].astype(jnp.bfloat16)

    before.wait_send()
    for c in range(chunks):
        chunk_copy(c, out_t, in_t, disp_send, disp_recv).wait_send()
        chunk_copy(c, ret_t, got_t, ret_send, ret_recv).wait_send()
        for copy in (ag_up, ag_dn, ag_up2, ag_dn2, rs_far_up, rs_far_dn, rs_own_up, rs_own_dn, rs_sum_up, rs_sum_dn):
            copy(c).wait_send()


def both_parts(queries, keys_values, sinks, tokens_b, norm_gain, routes, route_weights, wg, wu, wd):
    tokens, width = tokens_b.shape
    kv_rows = keys_values.shape[0]
    ffl = wg.shape[1]
    ep_size = lax.axis_size("ep")
    nz = ep_size // (NX * NC)
    chunks = max(1, nz // 2)
    rows = ep_size // chunks * CAP
    unit = width // LANES
    all_t = ep_size * CAP * unit
    half = width // 2
    bf, f32 = jnp.bfloat16, jnp.float32
    vmem = pl.BlockSpec(memory_space=pltpu.VMEM)
    hbm = pl.BlockSpec(memory_space=pl.ANY)
    dma = pltpu.SemaphoreType.DMA
    return pl.pallas_call(
        functools.partial(layer_kernel, nz),
        out_shape=(jax.ShapeDtypeStruct((tokens, width), bf), jax.ShapeDtypeStruct(queries.shape, bf)),
        in_specs=[vmem] * 4 + [pl.BlockSpec(memory_space=pltpu.SMEM)] + [hbm] * 5,
        out_specs=(vmem, vmem),
        scratch_shapes=[
            pltpu.VMEM((tokens, width), bf),
            pltpu.VMEM((rows * unit, LANES), f32),
            pltpu.VMEM((all_t, LANES), bf),
            pltpu.VMEM((all_t, LANES), bf),
            pltpu.VMEM((chunks, N_TP, rows, width), bf),
            pltpu.VMEM((width, ffl), bf),
            pltpu.VMEM((width, ffl), bf),
            pltpu.VMEM((ffl, width), bf),
            pltpu.VMEM((N_TP * rows, ffl), bf),
            pltpu.VMEM((chunks, N_TP, rows, width), bf),
            pltpu.VMEM((chunks, rows, half), bf),
            pltpu.VMEM((chunks, rows, half), bf),
            pltpu.VMEM((chunks, rows, half), bf),
            pltpu.VMEM((chunks, rows, half), bf),
            pltpu.VMEM((chunks, 2, rows, half), bf),
            pltpu.VMEM((chunks, 2, rows, half), bf),
            pltpu.VMEM((all_t, LANES), bf),
            pltpu.VMEM((all_t, LANES), bf),
            pltpu.VMEM((rows, width), bf),
            pltpu.VMEM((tokens, width), f32),
            pltpu.VMEM(queries.shape, bf),
            pltpu.VMEM((kv_rows + WINDOW, LANES), bf),
            pltpu.VMEM((2, kv_rows + WINDOW, LANES), bf),
            pltpu.VMEM((2, kv_rows + WINDOW, LANES), bf),
            dma((5,)), dma, dma,
            dma((chunks,)), dma((chunks,)), dma((chunks,)), dma((chunks,)),
            dma((4 * chunks,)), dma((4 * chunks,)), dma((6 * chunks,)), dma((6 * chunks,)),
        ],
        compiler_params=pltpu.CompilerParams(
            collective_id=0, has_side_effects=True, vmem_limit_bytes=60 * 1024 * 1024
        ),
        name="layer",
    )(
        tokens_b, norm_gain[None, :], routes.T, route_weights.T, sinks, queries,
        keys_values.reshape(kv_rows, LANES), wg, wu, wd,
    )


def local(
    queries, keys_values, sinks, tokens_b, norm_gain, routes, route_weights, gate_weight, up_weight, down_weight
):
    moe_out, attended = both_parts(
        queries, keys_values, sinks, tokens_b, norm_gain, routes, route_weights,
        gate_weight[0], up_weight[0], down_weight[0],
    )
    return (attended, moe_out)


def solution(mesh):
    in_specs = (
        P("ep", "tp"),
        P("ep", "tp", None),
        P("tp"),
        P(("ep", "tp"), None),
        P(),
        P(("ep", "tp"), None),
        P(("ep", "tp"), None),
        P("ep", None, "tp"),
        P("ep", None, "tp"),
        P("ep", "tp", None),
    )
    out_specs = (P("ep", "tp"), P(("ep", "tp"), None))
    return jax.shard_map(local, mesh=mesh, in_specs=in_specs, out_specs=out_specs, check_vma=False)
```

time: 335 us -> 132 us (0.39)
  waiting for transfers between devices: 147 us -> 0 us
  Pallas kernels: 0 us -> 127 us
  blocking collectives: 62.5 us -> 0 us
  local copies, waits for them, and re-layouts: 41.7 us -> 3.75 us
  matrix products: 31.8 us -> 0 us
  starting transfers between devices: 21.1 us -> 0 us
  other arithmetic: 14.7 us -> 0 us
  between operations: 14.3 us -> 0.64 us
    pallas_call x0 -> x1, Pallas kernels: none -> 127 us  [both_parts(): pl.pallas_call(functools.partial(layer_kernel, nz), out_shape=(jax.ShapeD...]
    all_to_all x2 -> x0, waiting for transfers between devices: 89.7 us -> none  [the longest x1 54.5 us: sent_and_summed(): lax.all_to_all(parts, axis, split_axis=0, concat_axis=0, tiled=True)]
    all_to_all x1 -> x0, blocking collectives: 62.5 us -> none  [local(): lax.all_to_all(outgoing, 'ep', split_axis=0, concat_axis=0, tiled=True)]
    all_gather x1 -> x0, waiting for transfers between devices: 57.3 us -> none  [local(): piece = lax.all_gather(arrived, 'tp', axis=0, tiled=True)]
    dot_general x4 -> x0, matrix products: 31.8 us -> none  [the longest x1 17.5 us: local(): jnp.dot(hidden, down_local, preferred_element_type=jnp.float32)]
    all_to_all x2 -> x0, starting transfers between devices: 17.2 us -> none  [the longest x1 12 us: local(): lax.all_to_all(summed.reshape(-1, capacity, model_width), 'ep', split_axi...]
    reshape x6 -> x0, local copies, waits for them, and re-layouts: 13.9 us -> none  [the longest x1 10 us: local(): flat_rows = piece.reshape(-1, model_width)]
    reduce_sum x5 -> x0, other arithmetic: 9.97 us -> none  [the longest x1 3.93 us: local(): moe_out = jnp.sum(weighted, axis=1).astype(jnp.bfloat16)]
  transfers between devices with their start and end apart: 4 -> 0, of which waited for: 3 -> 0; matrix products, arithmetic and copies ran while one was open for 6% -> 0% of each run, Pallas kernels for 0% -> 0%
where the time goes in v1:
time: 132 us
  Pallas kernels  127 us (96%)
  local copies, waits for them, and re-layouts  3.75 us (3%)
    pallas_call x1, Pallas kernels, both_parts(): pl.pallas_call(functools.partial(layer_kernel, nz), out_shape=(jax.ShapeD...  127 us
    unnamed x2, local copies, waits for them, and re-layouts  3.75 us

profile of v1, /device:TPU:1, one launch (start us, length us, event | category | flops | bytes accessed | tf_op | source)
XLA Modules:
  0.0 131.9 jit_solution(15364276755260541372)
XLA Ops:
  0.6 127.5 %layer.1 = (bf16[128,2048]{1,0:T(8,128)(2,1)}, bf16[512,512]{1,0:T(8,128)(2,1)}) custom-call(bf16[128,2048]{1,0:T(8,128)(2,1)} %tokens_ref.1, f32[1,2048]{1,0:T(1,128)} %bitcast.11, s32[2,128]{1,0:T(2,128)} %bitcast.12, f32[2,128]{1,0:T(2,128)} %bitcast.13, f32[8]{0:T(128)} %sinks_ref.1, bf16[512,512]{1,0:T(8,128)(2,1)} %q_hbm.1, bf16[512,128]{1,0:T(8,128)(2,1)} %bitcast.10, ...), custom_call_target="tpu_custom_call" | custom-call | tf_op jit(solution)/shard_map/layer/pallas_call | solution.py:404
  128.1 1.9 %copy.14 = bf16[512,512]{1,0:T(8,128)(2,1)} copy(bf16[512,512]{1,0:T(8,128)(2,1)} %get-tuple-element.8) | data formatting | bytes 1048576
  130.0 1.9 %copy.15 = bf16[128,2048]{1,0:T(8,128)(2,1)} copy(bf16[128,2048]{1,0:T(8,128)(2,1)} %get-tuple-element.9) | data formatting | bytes 1048576
